TPU v7x, 32 devices: a whole 2x2x4 slice. The times are simulated.
32 devices in a mesh: sp: 32 (over z, y, x, core), tp: 1.
Axes of the slice: x: 2, y: 2, z: 4, core: 2. Of those that a mesh axis runs over, the one named last changes fastest.
Arguments:
- stream: bfloat16 [8192, 2048], P(('sp', 'tp')), may hold values from -6 to 6
- query_one: bfloat16 [8192, 512], P('sp', 'tp'), may hold values from -280 to 280
- key_one: bfloat16 [8192, 512], P('sp', 'tp'), may hold values from -6 to 6
- query_two: bfloat16 [8192, 512], P('sp', 'tp'), may hold values from -280 to 280
- key_two: bfloat16 [8192, 512], P('sp', 'tp'), may hold values from -6 to 6
- values: bfloat16 [8192, 1024], P('sp', 'tp'), may hold values from -6 to 6
- lambdas: float32 [8], P('tp'), may hold values from 0.3 to 0.8
- head_gain: float32 [128], replicated, may hold values from 0.1 to 1.9
- out_weight: bfloat16 [1024, 2048], replicated, may hold values from -0.1875 to 0.1875
- norm_gain: float32 [2048], replicated, may hold values from 0.1 to 1.9
- gate_weight: bfloat16 [2048, 2816], P('sp', 'tp'), may hold values from -0.125 to 0.125
- up_weight: bfloat16 [2048, 2816], P('sp', 'tp'), may hold values from -0.125 to 0.125
- down_weight: bfloat16 [2816, 2048], P('tp', 'sp'), may hold values from -0.3125 to 0.3125
Outputs:
- result: bfloat16 [8192, 2048], P(('sp', 'tp'))
All inputs are finite; a program needn't handle non-finite values.
Results may differ from a plain program's by a relative error of at most 0.014.
Values may be sent and summed in bfloat16 or wider, within the bound.
A program may use at most 192 MiB of HBM per device.

v0:
```python
import math

import jax
import jax.numpy as jnp
from jax import lax
from jax.sharding import PartitionSpec as P

HEAD_DIM = 64


ALPHA = 1.4142135623730951
EPSILON = 1e-05


def update(carried, queries, keys, value_rows, factor):
    maxima, totals, weighted = carried
    scores = jnp.einsum("qhd,khd->hqk", queries, keys, preferred_element_type=jnp.float32) * factor
    new_maxima = jnp.maximum(maxima, jnp.max(scores, axis=-1))
    rescale = jnp.exp(maxima - new_maxima)
    weights = jnp.exp(scores - new_maxima[:, :, None])
    totals = totals * rescale + jnp.sum(weights, axis=-1)
    weighted = weighted * jnp.transpose(rescale)[:, :, None] + jnp.einsum(
        "hqk,khe->qhe", weights.astype(jnp.bfloat16), value_rows, preferred_element_type=jnp.float32
    )
    return (new_maxima, totals, weighted)


def finish(carried):
    maxima, totals, weighted = carried
    return weighted / jnp.transpose(totals)[:, :, None]


def layer_normed(heads_rows, residual_rows, out_weight, norm_gain):
    branch = jnp.dot(heads_rows, out_weight, preferred_element_type=jnp.float32)
    mixed_in = ALPHA * residual_rows.astype(jnp.float32) + branch
    row_mean = jnp.mean(mixed_in, axis=-1, keepdims=True)
    centered = mixed_in - row_mean
    row_var = jnp.mean(centered * centered, axis=-1, keepdims=True)
    return (centered * lax.rsqrt(row_var + EPSILON) * norm_gain).astype(jnp.bfloat16)


def sectioned_length(shard_len, group):
    return shard_len * math.gcd(128 // shard_len, group)


def sectioned_absorb(state, pieces, offset, along, block_len, work):
    running, sectioning, filled = state
    length = pieces[0].shape[along]
    sectioning = tuple((piece for piece in pieces))
    block_starts = jnp.arange(filled.shape[0], dtype=jnp.int32) * block_len
    covered = jnp.minimum(offset + length, block_starts + block_len) - jnp.maximum(
        offset, block_starts
    )
    covered = jnp.clip(covered, 0, block_len)
    before = filled
    filled = covered
    completed = (filled == block_len) & (before < block_len)

    def visit_block(block_index, totals):
        begin_at = block_index * block_len

        def compute(inner):
            slices = tuple(
                (
                    lax.dynamic_slice_in_dim(holder, begin_at, block_len, along)
                    for holder in sectioning
                )
            )
            return work(inner, slices, begin_at)

        def unchanged(inner):
            return inner

        return lax.cond(completed[block_index], compute, unchanged, totals)

    running = lax.fori_loop(0, filled.shape[0], visit_block, running)
    return (running, sectioning, filled)


def on_device(
    stream,
    query_one,
    key_one,
    query_two,
    key_two,
    values,
    lambdas,
    head_gain,
    out_weight,
    norm_gain,
    gate_weight,
    up_weight,
    down_weight,
):
    local_heads = lambdas.shape[0]
    head_width = query_one.shape[1] // local_heads
    value_width = values.shape[1] // local_heads
    tokens = query_one.shape[0]
    group = lax.axis_size("sp")
    factor = HEAD_DIM ** (-0.5)
    gate_full, up_full = (
        lax.all_gather(gate_weight, "sp", axis=0, tiled=True),
        lax.all_gather(up_weight, "sp", axis=0, tiled=True),
    )
    queries_first = query_one.reshape(tokens, local_heads, head_width)
    queries_second = query_two.reshape(tokens, local_heads, head_width)
    initial = (
        jnp.full((local_heads, tokens), -1e30, jnp.float32),
        jnp.zeros((local_heads, tokens), jnp.float32),
        jnp.zeros((tokens, local_heads, value_width), jnp.float32),
    )
    first_keys = lax.all_gather(key_one, "sp", axis=0, tiled=True)
    second_keys = lax.all_gather(key_two, "sp", axis=0, tiled=True)
    value_rows = lax.all_gather(values, "sp", axis=0, tiled=True)
    length = first_keys.shape[0]
    block_len = length
    while block_len > 2048 and block_len % 2 == 0:
        block_len = block_len // 2
    first_keys = first_keys.reshape(length, local_heads, head_width)
    second_keys = second_keys.reshape(length, local_heads, head_width)
    value_rows = value_rows.reshape(length, local_heads, value_width)

    def advance(block_index, partial_value):
        begin_row = block_index * block_len
        keys_first = lax.dynamic_slice_in_dim(first_keys, begin_row, block_len, 0)
        keys_second = lax.dynamic_slice_in_dim(second_keys, begin_row, block_len, 0)
        block_values = lax.dynamic_slice_in_dim(value_rows, begin_row, block_len, 0)
        return (
            update(partial_value[0], queries_first, keys_first, block_values, factor),
            update(partial_value[1], queries_second, keys_second, block_values, factor),
        )

    first_state, second_state = lax.fori_loop(0, length // block_len, advance, (initial, initial))
    differ = finish(first_state) - lambdas[None, :, None] * finish(second_state)
    inverse_rms = lax.rsqrt(jnp.mean(differ * differ, axis=-1, keepdims=True) + EPSILON)
    attended = (
        (differ * inverse_rms * head_gain * 0.8)
        .astype(jnp.bfloat16)
        .reshape(tokens, local_heads * value_width)
    )
    by_rows = lax.all_to_all(attended, "tp", split_axis=0, concat_axis=1, tiled=True)
    own_normed = layer_normed(by_rows, stream, out_weight, norm_gain)
    normed_all = lax.all_gather(own_normed, "tp", axis=0, tiled=True)
    row_count = normed_all.shape[0]
    gate_out = jnp.dot(normed_all, gate_full, preferred_element_type=jnp.float32)
    upward = jnp.dot(normed_all, up_full, preferred_element_type=jnp.float32)
    hidden = (jax.nn.silu(gate_out) * upward).astype(jnp.bfloat16)
    column_width = down_weight.shape[1]
    columns_block = sectioned_length(column_width, group)

    def project_block(outputs, slices, begin_at):
        product = jnp.dot(hidden, slices[0], preferred_element_type=jnp.float32)
        return lax.dynamic_update_slice_in_dim(outputs, product, begin_at, 1)

    project_start = (
        jnp.zeros((row_count, column_width * group), jnp.float32),
        (jnp.zeros((down_weight.shape[0], column_width * group), jnp.bfloat16),),
        jnp.zeros((column_width * group // columns_block,), jnp.int32),
    )
    project_state = sectioned_absorb(
        project_start,
        (lax.all_gather(down_weight, "sp", axis=1, tiled=True),),
        jnp.int32(0),
        1,
        columns_block,
        project_block,
    )
    partial_terms = project_state[0]
    mixer_out = lax.psum_scatter(
        partial_terms.astype(jnp.bfloat16), "tp", scatter_dimension=0, tiled=True
    ).astype(jnp.float32)
    return (ALPHA * own_normed.astype(jnp.float32) + 0.5 * mixer_out).astype(jnp.bfloat16)


def solution(mesh):
    return jax.shard_map(
        on_device,
        mesh=mesh,
        in_specs=(
            P(("sp", "tp"), None),
            P("sp", "tp"),
            P("sp", "tp"),
            P("sp", "tp"),
            P("sp", "tp"),
            P("sp", "tp"),
            P("tp"),
            P(),
            P(),
            P(),
            P("sp", "tp"),
            P("sp", "tp"),
            P("tp", "sp"),
        ),
        out_specs=P(("sp", "tp"), None),
        check_vma=False,
    )
```

profile of v0, /device:TPU:0, one launch (start us, length us, event | category | flops | bytes accessed | tf_op | source)
XLA Modules:
  0.0 724.0 jit_solution(6272200042016041110)
XLA Ops:
  13.2 76.8 %all-gather.7.cloned.1.call-done = bf16[8192,512]{1,0:T(8,128)(2,1)} async-done(((bf16[256,512]{1,0:T(8,128)(2,1)}), bf16[8192,512]{1,0:T(8,128)(2,1)}) %all-gather.7.cloned.1.call-update) | async-done | bytes 8388624 | tf_op jit(solution)/shard_map/all_gather | solution.py:112
  90.0 11.9 %copy.25 = bf16[8192,512]{0,1:T(8,128)(2,1)} copy(bf16[8192,512]{1,0:T(8,128)(2,1)} %all-gather.7.cloned.1.call-done) | data formatting | bytes 16777216 | tf_op jit(solution)/shard_map/all_gather | solution.py:112
  101.9 66.6 %all-gather.11.cloned.1.call-done = bf16[8192,512]{1,0:T(8,128)(2,1)} async-done(((bf16[256,512]{1,0:T(8,128)(2,1)}), bf16[8192,512]{1,0:T(8,128)(2,1)}) %all-gather.11.cloned.1.call-update) | async-done | bytes 8388624 | tf_op jit(solution)/shard_map/all_gather | solution.py:113
  168.6 11.8 %copy.28 = bf16[8192,512]{0,1:T(8,128)(2,1)} copy(bf16[8192,512]{1,0:T(8,128)(2,1)} %all-gather.11.cloned.1.call-done) | data formatting | bytes 16777216 | tf_op jit(solution)/shard_map/all_gather | solution.py:113
  180.3 80.3 %all-gather.13.cloned.1.call-done = bf16[2816,2048]{0,1:T(8,128)(2,1)} async-done(((bf16[2816,64]{0,1:T(8,128)(2,1)}), bf16[2816,2048]{0,1:T(8,128)(2,1)}) %all-gather.13.cloned.1.call-update) | async-done | bytes 11534352 | tf_op jit(solution)/shard_map/all_gather | solution.py:162
  260.6 15.3 %copy.30 = bf16[2816,2048]{1,0:T(8,128)(2,1)} copy(bf16[2816,2048]{0,1:T(8,128)(2,1)} %all-gather.13.cloned.1.call-done) | data formatting | bytes 23068672 | tf_op jit(solution)/shard_map/while | solution.py:76
  275.9 100.4 %all-gather.9.cloned.1.call-done = bf16[8192,1024]{1,0:T(8,128)(2,1)} async-done(((bf16[256,1024]{1,0:T(8,128)(2,1)}), bf16[8192,1024]{1,0:T(8,128)(2,1)}) %all-gather.9.cloned.1.call-update) | async-done | bytes 16777232 | tf_op jit(solution)/shard_map/all_gather | solution.py:114
  376.3 21.3 %copy.27 = bf16[8192,1024]{0,1:T(8,128)(2,1)} copy(bf16[8192,1024]{1,0:T(8,128)(2,1)} %all-gather.9.cloned.1.call-done) | data formatting | bytes 33554432 | tf_op jit(solution)/shard_map/all_gather | solution.py:114
  397.6 225.1 %while.41 = (s32[]{:T(128)}, f32[8,256]{1,0:T(8,128)S(1)}, f32[8,256]{1,0:T(8,128)S(1)}, f32[256,8,128]{0,2,1:T(8,128)S(1)}, f32[8,256]{1,0:T(8,128)S(1)}, /*ind...) while((s32[]{:T(128)}, f32[8,256]{1,0:T(8,128)S(1)}, ...), condition=%wide.region_5.0_spmd.clone, body=%wide.region_0.0_spmd.clone.sunk | while | flops 3289931776 | bytes 118227160 | solution.py:133
  397.6 9.9 %bitcast_reduce_fusion.5 = (f32[8,256]{1,0:T(8,128)S(1)}, f32[8,2048,256]{2,1,0:T(8,128)}) fusion(bf16[256,8,64]{0,2,1:T(8,128)(2,1)S(1)} %get-tuple-element.595, bf16[8192,8,64]{0,2,1:T(8,128)(2,1)} %get-tuple-element.594, s32[]{:T(128)S(6)} %select_n.21), kind=kOutput, calls=%fused_computation.5.clone.1 | convolution fusion | flops 545257472 | bytes 19144708 | tf_op jit(solution)/shard_map/while/body/eval_jaxpr/qhd,khd->hqk/dot_general | solution.py:17
  407.5 9.2 %fusion.90 = f32[256,8,128]{0,2,1:T(8,128)S(1)} fusion(f32[8,2048,256]{2,1,0:T(8,128)} %get-tuple-element.544, f32[8,256]{1,0:T(8,128)S(1)} %get-tuple-element.588, bf16[8192,8,128]{0,2,1:T(8,128)(2,1)} %get-tuple-element.593, s32[]{:T(128)S(6)} %select_n.21, f32[256,8,128]{0,2,1:T(8,128)S(1)} %get-tuple-element.574, ...), kind=kOutput, calls=%fused_computation.28.clone.1 | convolution fusion | flops 1087111168 | bytes 23085060 | tf_op jit(solution)/shard_map/while/body/eval_jaxpr/hqk,khe->qhe/dot_general | solution.py:22
  416.7 9.7 %bitcast_reduce_fusion.4 = (f32[8,256]{1,0:T(8,128)S(1)}, f32[8,2048,256]{2,1,0:T(8,128)}) fusion(bf16[256,8,64]{0,2,1:T(8,128)(2,1)S(1)} %get-tuple-element.592, bf16[8192,8,64]{0,2,1:T(8,128)(2,1)} %get-tuple-element.591, s32[]{:T(128)S(6)} %select_n.21), kind=kOutput, calls=%fused_computation.8.clone.1 | convolution fusion | flops 545257472 | bytes 19144708 | tf_op jit(solution)/shard_map/while/body/eval_jaxpr/qhd,khd->hqk/dot_general | solution.py:17
  426.4 10.7 %fusion.89 = f32[256,8,128]{0,2,1:T(8,128)S(1)} fusion(f32[8,2048,256]{2,1,0:T(8,128)} %get-tuple-element.547, f32[8,256]{1,0:T(8,128)S(1)} %get-tuple-element.585, bf16[8192,8,128]{0,2,1:T(8,128)(2,1)} %get-tuple-element.593, s32[]{:T(128)S(6)} %select_n.21, f32[256,8,128]{0,2,1:T(8,128)S(1)} %get-tuple-element.571, ...), kind=kOutput, calls=%fused_computation.29.clone.1 | convolution fusion | flops 1087111168 | bytes 23085060 | tf_op jit(solution)/shard_map/while/body/eval_jaxpr/hqk,khe->qhe/dot_general | solution.py:22
  454.5 10.0 %bitcast_reduce_fusion.5 = (f32[8,256]{1,0:T(8,128)S(1)}, f32[8,2048,256]{2,1,0:T(8,128)}) fusion(bf16[256,8,64]{0,2,1:T(8,128)(2,1)S(1)} %get-tuple-element.595, bf16[8192,8,64]{0,2,1:T(8,128)(2,1)} %get-tuple-element.594, s32[]{:T(128)S(6)} %select_n.21), kind=kOutput, calls=%fused_computation.5.clone.1 | convolution fusion | flops 545257472 | bytes 19144708 | tf_op jit(solution)/shard_map/while/body/eval_jaxpr/qhd,khd->hqk/dot_general | solution.py:17
  464.4 9.5 %fusion.90 = f32[256,8,128]{0,2,1:T(8,128)S(1)} fusion(f32[8,2048,256]{2,1,0:T(8,128)} %get-tuple-element.544, f32[8,256]{1,0:T(8,128)S(1)} %get-tuple-element.588, bf16[8192,8,128]{0,2,1:T(8,128)(2,1)} %get-tuple-element.593, s32[]{:T(128)S(6)} %select_n.21, f32[256,8,128]{0,2,1:T(8,128)S(1)} %get-tuple-element.574, ...), kind=kOutput, calls=%fused_computation.28.clone.1 | convolution fusion | flops 1087111168 | bytes 23085060 | tf_op jit(solution)/shard_map/while/body/eval_jaxpr/hqk,khe->qhe/dot_general | solution.py:22
  474.0 9.7 %bitcast_reduce_fusion.4 = (f32[8,256]{1,0:T(8,128)S(1)}, f32[8,2048,256]{2,1,0:T(8,128)}) fusion(bf16[256,8,64]{0,2,1:T(8,128)(2,1)S(1)} %get-tuple-element.592, bf16[8192,8,64]{0,2,1:T(8,128)(2,1)} %get-tuple-element.591, s32[]{:T(128)S(6)} %select_n.21), kind=kOutput, calls=%fused_computation.8.clone.1 | convolution fusion | flops 545257472 | bytes 19144708 | tf_op jit(solution)/shard_map/while/body/eval_jaxpr/qhd,khd->hqk/dot_general | solution.py:17
  483.7 9.2 %fusion.89 = f32[256,8,128]{0,2,1:T(8,128)S(1)} fusion(f32[8,2048,256]{2,1,0:T(8,128)} %get-tuple-element.547, f32[8,256]{1,0:T(8,128)S(1)} %get-tuple-element.585, bf16[8192,8,128]{0,2,1:T(8,128)(2,1)} %get-tuple-element.593, s32[]{:T(128)S(6)} %select_n.21, f32[256,8,128]{0,2,1:T(8,128)S(1)} %get-tuple-element.571, ...), kind=kOutput, calls=%fused_computation.29.clone.1 | convolution fusion | flops 1087111168 | bytes 23085060 | tf_op jit(solution)/shard_map/while/body/eval_jaxpr/hqk,khe->qhe/dot_general | solution.py:22
  510.4 9.7 %bitcast_reduce_fusion.5 = (f32[8,256]{1,0:T(8,128)S(1)}, f32[8,2048,256]{2,1,0:T(8,128)}) fusion(bf16[256,8,64]{0,2,1:T(8,128)(2,1)S(1)} %get-tuple-element.595, bf16[8192,8,64]{0,2,1:T(8,128)(2,1)} %get-tuple-element.594, s32[]{:T(128)S(6)} %select_n.21), kind=kOutput, calls=%fused_computation.5.clone.1 | convolution fusion | flops 545257472 | bytes 19144708 | tf_op jit(solution)/shard_map/while/body/eval_jaxpr/qhd,khd->hqk/dot_general | solution.py:17
  520.1 10.8 %fusion.90 = f32[256,8,128]{0,2,1:T(8,128)S(1)} fusion(f32[8,2048,256]{2,1,0:T(8,128)} %get-tuple-element.544, f32[8,256]{1,0:T(8,128)S(1)} %get-tuple-element.588, bf16[8192,8,128]{0,2,1:T(8,128)(2,1)} %get-tuple-element.593, s32[]{:T(128)S(6)} %select_n.21, f32[256,8,128]{0,2,1:T(8,128)S(1)} %get-tuple-element.574, ...), kind=kOutput, calls=%fused_computation.28.clone.1 | convolution fusion | flops 1087111168 | bytes 23085060 | tf_op jit(solution)/shard_map/while/body/eval_jaxpr/hqk,khe->qhe/dot_general | solution.py:22
  530.9 9.7 %bitcast_reduce_fusion.4 = (f32[8,256]{1,0:T(8,128)S(1)}, f32[8,2048,256]{2,1,0:T(8,128)}) fusion(bf16[256,8,64]{0,2,1:T(8,128)(2,1)S(1)} %get-tuple-element.592, bf16[8192,8,64]{0,2,1:T(8,128)(2,1)} %get-tuple-element.591, s32[]{:T(128)S(6)} %select_n.21), kind=kOutput, calls=%fused_computation.8.clone.1 | convolution fusion | flops 545257472 | bytes 19144708 | tf_op jit(solution)/shard_map/while/body/eval_jaxpr/qhd,khd->hqk/dot_general | solution.py:17
  540.6 9.5 %fusion.89 = f32[256,8,128]{0,2,1:T(8,128)S(1)} fusion(f32[8,2048,256]{2,1,0:T(8,128)} %get-tuple-element.547, f32[8,256]{1,0:T(8,128)S(1)} %get-tuple-element.585, bf16[8192,8,128]{0,2,1:T(8,128)(2,1)} %get-tuple-element.593, s32[]{:T(128)S(6)} %select_n.21, f32[256,8,128]{0,2,1:T(8,128)S(1)} %get-tuple-element.571, ...), kind=kOutput, calls=%fused_computation.29.clone.1 | convolution fusion | flops 1087111168 | bytes 23085060 | tf_op jit(solution)/shard_map/while/body/eval_jaxpr/hqk,khe->qhe/dot_general | solution.py:22
  567.6 9.7 %bitcast_reduce_fusion.5 = (f32[8,256]{1,0:T(8,128)S(1)}, f32[8,2048,256]{2,1,0:T(8,128)}) fusion(bf16[256,8,64]{0,2,1:T(8,128)(2,1)S(1)} %get-tuple-element.595, bf16[8192,8,64]{0,2,1:T(8,128)(2,1)} %get-tuple-element.594, s32[]{:T(128)S(6)} %select_n.21), kind=kOutput, calls=%fused_computation.5.clone.1 | convolution fusion | flops 545257472 | bytes 19144708 | tf_op jit(solution)/shard_map/while/body/eval_jaxpr/qhd,khd->hqk/dot_general | solution.py:17
  586.5 9.7 %bitcast_reduce_fusion.4 = (f32[8,256]{1,0:T(8,128)S(1)}, f32[8,2048,256]{2,1,0:T(8,128)}) fusion(bf16[256,8,64]{0,2,1:T(8,128)(2,1)S(1)} %get-tuple-element.592, bf16[8192,8,64]{0,2,1:T(8,128)(2,1)} %get-tuple-element.591, s32[]{:T(128)S(6)} %select_n.21), kind=kOutput, calls=%fused_computation.8.clone.1 | convolution fusion | flops 545257472 | bytes 19144708 | tf_op jit(solution)/shard_map/while/body/eval_jaxpr/qhd,khd->hqk/dot_general | solution.py:17
  646.9 67.1 %while.40 = (s32[]{:T(128)}, bf16[256,2048]{0,1:T(8,128)(2,1)}, pred[16]{0:T(512)(128)(4,1)}, bf16[2816,2048]{1,0:T(8,128)(2,1)}, bf16[256,2816]{1,0:T(8,128)(2,1)S(1)}, /*index=5*/s32[]{:T(128)}) while((s32[]{:T(128)}, bf16[256,2048]{0,1:T(8,128)(2,1)}, pred[16]{0:T(512)(128)(4,1)}, bf16[2816,2048]{1,0:T(8,128)(2,1)}, ...), condition=%wide.region_12.13_spmd, body=%wide.region_9.12_spmd.sunk | while | flops 184549376 | bytes 2294950 | solution.py:76
  (121 shorter events, 216.5 us)
Async XLA Ops:
  6.5 83.5 %all-gather.7.cloned.1.call-start = ((), (), s32[]{:S(2)}) async-start(), calls=%async_computation | async-start | bytes 8650752 | tf_op jit(solution)/shard_map/all_gather | solution.py:112
  7.3 161.3 %all-gather.11.cloned.1.call-start = ((), (), s32[]{:S(2)}) async-start(), calls=%async_computation.2 | async-start | bytes 8650752 | tf_op jit(solution)/shard_map/all_gather | solution.py:113
  8.0 252.6 %all-gather.13.cloned.1.call-start = ((), (), s32[]{:S(2)}) async-start(), calls=%async_computation.3 | async-start | bytes 11894784 | tf_op jit(solution)/shard_map/all_gather | solution.py:162
  8.7 367.5 %all-gather.9.cloned.1.call-start = ((), (), s32[]{:S(2)}) async-start(), calls=%async_computation.1 | async-start | bytes 17301504 | tf_op jit(solution)/shard_map/all_gather | solution.py:114
  9.3 618.6 %all-gather.15.cloned.1.call-start = ((), (), s32[]{:S(2)}) async-start(), calls=%async_computation.4 | async-start | bytes 11894784 | tf_op jit(solution)/shard_map/all_gather | solution.py:102
  9.9 627.1 %all-gather.17.cloned.1.call-start = ((), (), s32[]{:S(2)}) async-start(), calls=%async_computation.5 | async-start | bytes 11894784 | tf_op jit(solution)/shard_map/all_gather | solution.py:103
  397.6 225.1 %copy-start.3 = (f32[8]{0:T(128)S(1)}, f32[8]{0:T(128)}, u32[]{:S(2)}) copy-start(f32[8]{0:T(128)} %param.25) | copy-start | bytes 100
  397.6 225.4 %copy-start.2 = (f32[128]{0:T(128)S(1)}, f32[128]{0:T(128)}, u32[]{:S(2)}) copy-start(f32[128]{0:T(128)} %param.26) | copy-start | bytes 1540
  622.7 2.2 copy-start
  624.9 3.0 copy-start.1
Sparse Core Ops, SparseCore 0:
  10.2 79.7 all-gather.6
  92.8 75.6 all-gather.10
  171.4 89.1 all-gather.12
  263.3 112.9 all-gather.8
  379.0 88.7 all-gather.14
  470.5 89.1 all-gather.16
where the time goes:
time: 727 us; the launch traced here: 724 us
  waiting for transfers between devices  328 us (45%)
  matrix products  214 us (29%)
  local copies, waits for them, and re-layouts  85.4 us (12%)
  other arithmetic  72.1 us (10%)
  between operations  13.6 us (2%)
  loops' own time  10.8 us (1%)
    all_gather x1, waiting for transfers between devices, on_device(): value_rows = lax.all_gather(values, 'sp', axis=0, tiled=True)  100 us
    all_gather x1, waiting for transfers between devices, on_device(): lax.all_gather(down_weight, 'sp', axis=1, tiled=True)  80.3 us
    dot_general x8, matrix products, update(): jnp.einsum('qhd,khd->hqk', queries, keys, preferred_element_type=jnp.floa...  78.1 us
    dot_general x8, matrix products, update(): jnp.einsum('hqk,khe->qhe', weights.astype(jnp.bfloat16), value_rows, pref...  77.3 us
    all_gather x1, waiting for transfers between devices, on_device(): first_keys = lax.all_gather(key_one, 'sp', axis=0, tiled=True)  76.8 us
    reduce_sum x8, other arithmetic, update(): totals = totals * rescale + jnp.sum(weights, axis=-1)  69.1 us
    all_gather x1, waiting for transfers between devices, on_device(): second_keys = lax.all_gather(key_two, 'sp', axis=0, tiled=True)  66.6 us
    dot_general x16, matrix products, project_block(): product = jnp.dot(hidden, slices[0], preferred_element_type=jnp.float32)  38.1 us
  transfers between devices with their start and end apart: 6, of which 4 were waited for; matrix products, arithmetic and copies ran while one was open for 41% of the time, Pallas kernels for 0%

commit v1 on v0

v1 whole, which is shorter than its diff:
```python
import functools

import jax
import jax.numpy as jnp
from jax import lax
from jax.experimental import pallas as pl
from jax.experimental.pallas import tpu as pltpu
from jax.sharding import PartitionSpec as P

ALPHA = 1.4142135623730951
EPSILON = 1e-05


def attend_kernel(first, last, factor, block_keys, *refs):
    refs = list(refs)
    lam_ref, gain_ref, q_ref, kv_ref = refs[:4]
    refs = refs[4:]
    if not first:
        m_in, acc_in = refs[:2]
        refs = refs[2:]
    if last:
        (out_ref,) = refs[:1]
        refs = refs[1:]
    else:
        m_out, acc_out = refs[:2]
        refs = refs[2:]
    (vext,) = refs
    rows, width = q_ref.shape
    head = width // 2
    keys = kv_ref.shape[0]
    vdim = kv_ref.shape[1] - width

    @pl.when(pl.program_id(0) == 0)
    def _():
        vext[:, :vdim] = kv_ref[:, width:]
        vext[:, vdim:] = jnp.ones((keys, vdim), vext.dtype)

    q = q_ref[...] * jnp.asarray(factor, q_ref.dtype)
    lane = lax.broadcasted_iota(jnp.int32, q.shape, 1)
    zero = jnp.zeros_like(q)
    maps = [jnp.where(lane < head, q, zero), jnp.where(lane < head, zero, q)]
    ms, accs = [], []
    for i in range(2):
        if first:
            ms.append(jnp.full((rows, 1), -1e30, jnp.float32))
            accs.append(None)
        else:
            ms.append(m_in[i][:, :1])
            accs.append(acc_in[i])
    for start in range(0, keys, block_keys):
        kk = kv_ref[start : start + block_keys, :width]
        vv = vext[start : start + block_keys, :]
        for i in range(2):
            s = lax.dot_general(maps[i], kk, (((1,), (1,)), ((), ())), preferred_element_type=jnp.float32)
            m_new = jnp.maximum(ms[i], jnp.max(s, axis=1, keepdims=True))
            p = jnp.exp(s - m_new).astype(jnp.bfloat16)
            pv = jnp.dot(p, vv, preferred_element_type=jnp.float32)
            if accs[i] is None:
                accs[i] = pv
            else:
                accs[i] = accs[i] * jnp.exp(ms[i] - m_new) + pv
            ms[i] = m_new
    if last:
        o = [a[:, :vdim] / a[:, vdim:] for a in accs]
        differ = o[0] - lam_ref[0] * o[1]
        inverse = lax.rsqrt(jnp.mean(differ * differ, axis=1, keepdims=True) + EPSILON)
        out_ref[...] = (differ * inverse * gain_ref[...] * 0.8).astype(out_ref.dtype)
    else:
        for i in range(2):
            m_out[i] = jnp.broadcast_to(ms[i], (rows, m_out.shape[2]))
            acc_out[i] = accs[i]


def attend(lam, gain, q, kv, state, last, factor):
    rows, width = q.shape
    keys = kv.shape[0]
    vdim = kv.shape[1] - width
    block = min(256, rows)
    first = state is None
    smem = pl.BlockSpec(memory_space=pltpu.SMEM)
    m_spec = pl.BlockSpec((2, block, 128), lambda i: (0, i, 0))
    acc_spec = pl.BlockSpec((2, block, 2 * vdim), lambda i: (0, i, 0))
    in_specs = [
        smem,
        pl.BlockSpec((1, vdim), lambda i: (0, 0)),
        pl.BlockSpec((block, width), lambda i: (i, 0)),
        pl.BlockSpec((keys, width + vdim), lambda i: (0, 0)),
    ]
    args = [lam, gain, q, kv]
    aliases = {}
    if not first:
        in_specs += [m_spec, acc_spec]
        args += list(state)
        if not last:
            aliases = {4: 0, 5: 1}
    if last:
        out_shape = jax.ShapeDtypeStruct((rows, vdim), jnp.bfloat16)
        out_specs = pl.BlockSpec((block, vdim), lambda i: (i, 0))
    else:
        out_shape = (
            jax.ShapeDtypeStruct((2, rows, 128), jnp.float32),
            jax.ShapeDtypeStruct((2, rows, 2 * vdim), jnp.float32),
        )
        out_specs = (m_spec, acc_spec)
    return pl.pallas_call(
        functools.partial(attend_kernel, first, last, factor, min(1024, keys)),
        grid=(rows // block,),
        in_specs=in_specs,
        out_specs=out_specs,
        out_shape=out_shape,
        input_output_aliases=aliases,
        scratch_shapes=[pltpu.VMEM((keys, 2 * vdim), jnp.bfloat16)],
        compiler_params=pltpu.CompilerParams(dimension_semantics=("arbitrary",)),
    )(*args)


def layer_normed(heads_rows, residual_rows, out_weight, norm_gain):
    branch = jnp.dot(heads_rows, out_weight, preferred_element_type=jnp.float32)
    mixed_in = ALPHA * residual_rows.astype(jnp.float32) + branch
    row_mean = jnp.mean(mixed_in, axis=-1, keepdims=True)
    centered = mixed_in - row_mean
    row_var = jnp.mean(centered * centered, axis=-1, keepdims=True)
    return (centered * lax.rsqrt(row_var + EPSILON) * norm_gain).astype(jnp.bfloat16)


def on_device(
    stream,
    query_one,
    key_one,
    query_two,
    key_two,
    values,
    lambdas,
    head_gain,
    out_weight,
    norm_gain,
    gate_weight,
    up_weight,
    down_weight,
):
    heads = lambdas.shape[0]
    tokens = query_one.shape[0]
    head_width = query_one.shape[1] // heads
    vdim = values.shape[1] // heads
    hidden_units = gate_weight.shape[1]
    group = lax.axis_size("sp")
    tp = lax.axis_size("tp")
    ring = group // heads
    me = lax.axis_index("sp")
    factor = head_width ** (-0.5)

    packed = jnp.concatenate([gate_weight, up_weight, down_weight.T], axis=1)
    weights = lax.all_gather(packed, "sp", axis=0, tiled=True)

    def by_head(a):
        return jnp.transpose(a.reshape(tokens, heads, a.shape[1] // heads), (1, 0, 2))

    own = jnp.concatenate([by_head(a) for a in (query_one, query_two, key_one, key_two, values)], axis=2)
    near = [[r * heads + h for h in range(heads)] for r in range(ring)]
    mine = lax.all_to_all(own, "sp", split_axis=0, concat_axis=0, axis_index_groups=near, tiled=True)
    mine = mine.reshape(heads * tokens, own.shape[2])
    q = mine[:, : 2 * head_width]
    kv = mine[:, 2 * head_width :]
    lam = lax.dynamic_slice_in_dim(lambdas, lax.rem(me, heads), 1, 0)
    gain = head_gain.reshape(1, vdim)
    onward = [(d, (d + heads) % group) for d in range(group)]
    state = None
    for step in range(ring):
        following = lax.ppermute(kv, "sp", onward) if step + 1 < ring else None
        state = attend(lam, gain, q, kv, state, step + 1 == ring, factor)
        kv = following
    back = lax.all_to_all(
        state.reshape(heads, tokens, vdim), "sp", split_axis=0, concat_axis=0, axis_index_groups=near, tiled=True
    )
    attended = jnp.transpose(back, (1, 0, 2)).reshape(tokens, heads * vdim)

    by_rows = lax.all_to_all(attended, "tp", split_axis=0, concat_axis=1, tiled=True) if tp > 1 else attended
    own_normed = layer_normed(by_rows, stream, out_weight, norm_gain)
    normed_all = lax.all_gather(own_normed, "tp", axis=0, tiled=True) if tp > 1 else own_normed
    gate_out = jnp.dot(normed_all, weights[:, :hidden_units], preferred_element_type=jnp.float32)
    upward = jnp.dot(normed_all, weights[:, hidden_units : 2 * hidden_units], preferred_element_type=jnp.float32)
    hidden = (jax.nn.silu(gate_out) * upward).astype(jnp.bfloat16)
    partial_terms = lax.dot_general(
        hidden, weights[:, 2 * hidden_units :], (((1,), (1,)), ((), ())), preferred_element_type=jnp.float32
    ).astype(jnp.bfloat16)
    if tp > 1:
        partial_terms = lax.psum_scatter(partial_terms, "tp", scatter_dimension=0, tiled=True)
    mixer_out = partial_terms.astype(jnp.float32)
    return (ALPHA * own_normed.astype(jnp.float32) + 0.5 * mixer_out).astype(jnp.bfloat16)


def solution(mesh):
    return jax.shard_map(
        on_device,
        mesh=mesh,
        in_specs=(
            P(("sp", "tp"), None),
            P("sp", "tp"),
            P("sp", "tp"),
            P("sp", "tp"),
            P("sp", "tp"),
            P("sp", "tp"),
            P("tp"),
            P(),
            P(),
            P(),
            P("sp", "tp"),
            P("sp", "tp"),
            P("tp", "sp"),
        ),
        out_specs=P(("sp", "tp"), None),
        check_vma=False,
    )
```

time: 727 us -> 304 us (0.42)
  waiting for transfers between devices: 328 us -> 115 us
  matrix products: 214 us -> 26.6 us
  local copies, waits for them, and re-layouts: 85.4 us -> 10.6 us
  Pallas kernels: 0 us -> 73.4 us
  other arithmetic: 72.1 us -> 2.76 us
  blocking collectives: 0 us -> 47.2 us
  starting transfers between devices: 0.19 us -> 13.5 us
  loops' own time: 10.8 us -> 0 us
    all_gather x6 -> x1, waiting for transfers between devices: 324 us -> 29.4 us  [on_device(): weights = lax.all_gather(packed, 'sp', axis=0, tiled=True)]
    dot_general x34 -> x2, matrix products: 211 us -> 22.7 us  [the longest x1 13.6 us: on_device(): lax.dot_general(hidden, weights[:, 2 * hidden_units:], (((1,), (1,)), (()...]
    ppermute x0 -> x3, waiting for transfers between devices: none -> 85.7 us  [on_device(): following = lax.ppermute(kv, 'sp', onward) if step + 1 < ring else None]
    pallas_call x0 -> x4, Pallas kernels: none -> 73.4 us  [attend(): pl.pallas_call(functools.partial(attend_kernel, first, last, factor, min(...]
    reduce_sum x9 -> x0, other arithmetic: 69.3 us -> none  [the longest x8 69.1 us: update(): totals = totals * rescale + jnp.sum(weights, axis=-1)]
    all_to_all x0 -> x2, blocking collectives: none -> 47.2 us  [the longest x1 33.7 us: on_device(): lax.all_to_all(own, 'sp', split_axis=0, concat_axis=0, axis_index_groups=...]
    all_gather x3 -> x0, local copies, waits for them, and re-layouts: 45 us -> none  [the longest x1 21.3 us: on_device(): value_rows = lax.all_gather(values, 'sp', axis=0, tiled=True)]
    dynamic_slice x16 -> x1, local copies, waits for them, and re-layouts: 18.6 us -> 0.59 us  [on_device(): lam = lax.dynamic_slice_in_dim(lambdas, lax.rem(me, heads), 1, 0)]
  transfers between devices with their start and end apart: 6 -> 4, of which waited for: 4 -> 3; matrix products, arithmetic and copies ran while one was open for 41% -> 5% of each run, Pallas kernels for 0% -> 24%
where the time goes in v1:
time: 304 us; the launch traced here: 303 us
  waiting for transfers between devices  115 us (38%)
  Pallas kernels  73.4 us (24%)
  blocking collectives  47.2 us (16%)
  matrix products  26.6 us (9%)
  starting transfers between devices  13.5 us (4%)
  between operations  13.5 us (4%)
  local copies, waits for them, and re-layouts  10.6 us (3%)
    ppermute x3, waiting for transfers between devices, on_device(): following = lax.ppermute(kv, 'sp', onward) if step + 1 < ring else None  85.7 us
    pallas_call x4, Pallas kernels, attend(): pl.pallas_call(functools.partial(attend_kernel, first, last, factor, min(...  73.4 us
    all_to_all x1, blocking collectives, on_device(): lax.all_to_all(own, 'sp', split_axis=0, concat_axis=0, axis_index_groups=...  33.7 us
    all_gather x1, waiting for transfers between devices, on_device(): weights = lax.all_gather(packed, 'sp', axis=0, tiled=True)  29.4 us
    all_to_all x1, blocking collectives, on_device(): lax.all_to_all(state.reshape(heads, tokens, vdim), 'sp', split_axis=0, co...  13.6 us
    dot_general x1, matrix products, on_device(): lax.dot_general(hidden, weights[:, 2 * hidden_units:], (((1,), (1,)), (()...  13.6 us
    ppermute x3, starting transfers between devices, on_device(): following = lax.ppermute(kv, 'sp', onward) if step + 1 < ring else None  13.5 us
    dot_general x1, matrix products, on_device(): jnp.dot(normed_all, weights[:, :hidden_units], preferred_element_type=jnp...  9.13 us
  transfers between devices with their start and end apart: 4, of which 3 were waited for; matrix products, arithmetic and copies ran while one was open for 5% of the time, Pallas kernels for 24%

profile of v1, /device:TPU:0, one launch (start us, length us, event | category | flops | bytes accessed | tf_op | source)
XLA Modules:
  0.0 302.7 jit_solution(14878730764894862887)
XLA Ops:
  6.5 2.4 pad_maximum_fusion
  10.0 1.0 copy.30
  11.2 1.0 copy.31
  12.2 0.9 bitcast_bitcast_fusion
  13.1 2.8 concatenate.6
  15.9 33.7 %all_to_all.10 = bf16[8,256,384]{2,1,0:T(8,128)(2,1)S(1)} all-to-all(bf16[8,256,384]{2,1,0:T(8,128)(2,1)S(1)} %concatenate.6), channel_id=1, replica_groups={{0,1,2,3,4,5,6,7},{8,9,10,11,12,13,14,15},{16,17,18,19,20,21,22,23},{24..., dimensions={0} | all-to-all | bytes 3145728 | tf_op jit(solution)/shard_map/all_to_all | solution.py:160
  49.7 1.6 collective-permute-start
  51.3 37.9 %collective-permute-done.refs_3_ = bf16[2048,256]{1,0:T(8,128)(2,1)S(1)} collective-permute-done((bf16[2048,256]{1,0:T(8,128)(2,1)S(1)}, bf16[2048,256]{1,0:T(8,128)(2,1)S(1)}, u32[]{:S(2)}, u32[]{:S(2)}) %collective-permute-start) | collective-permute-done | bytes 1048608 | tf_op jit(solution)/shard_map/ppermute | solution.py:169
  89.2 1.0 copy-done.3
  90.1 2.7 collective-permute-start.1
  92.9 47.8 %collective-permute-done.1.refs_3_ = bf16[2048,256]{1,0:T(8,128)(2,1)} collective-permute-done((bf16[2048,256]{1,0:T(8,128)(2,1)S(1)}, bf16[2048,256]{1,0:T(8,128)(2,1)}, u32[]{:S(2)}, u32[]{:S(2)}) %collective-permute-start.1) | collective-permute-done | bytes 1048608 | tf_op jit(solution)/shard_map/ppermute | solution.py:169
  140.7 9.1 %collective-permute-start.2 = (bf16[2048,256]{1,0:T(8,128)(2,1)}, bf16[2048,256]{1,0:T(8,128)(2,1)}, u32[]{:S(2)}, u32[]{:S(2)}) collective-permute-start(bf16[2048,256]{1,0:T(8,128)(2,1)} %collective-permute-done.1.refs_3_), channel_id=1, source_target_pairs={{0,8},{1,9},{2,10},{3,11},{4,12},{5,13},{6,14},{7,15},{8,16},{9,17... | collective-permute-start | bytes 3145736 | tf_op jit(solution)/shard_map/ppermute | solution.py:169
  149.8 0.6 dynamic_slice.3.refs_0_
  150.4 0.8 slice.20.refs_2_
  151.3 16.8 %shard_map.127 = (f32[2,2048,128]{2,1,0:T(8,128)}, f32[2,2048,256]{2,1,0:T(8,128)}) custom-call(f32[1]{0:T(128)} %dynamic_slice.3.refs_0_, f32[1,128]{1,0:T(1,128)} %bitcast.37, bf16[2048,128]{1,0:T(8,128)(2,1)} %slice.20.refs_2_, bf16[2048,256]{1,0:T(8,128)(2,1)} %copy-done.2), custom_call_target="tpu_custom_call" | custom-call | tf_op jit(solution)/shard_map/pallas_call | solution.py:105
  168.0 18.8 %shard_map.128 = (f32[2,2048,128]{2,1,0:T(8,128)}, f32[2,2048,256]{2,1,0:T(8,128)}) custom-call(f32[1]{0:T(128)} %dynamic_slice.3.refs_0_, f32[1,128]{1,0:T(1,128)} %bitcast.38, bf16[2048,128]{1,0:T(8,128)(2,1)} %slice.20.refs_2_, bf16[2048,256]{1,0:T(8,128)(2,1)} %copy-done.3, ...), custom_call_target="tpu_custom_call", output_to_operand_aliasing={{0}: (4, {}), {1}: (5, {})} | custom-call | tf_op jit(solution)/shard_map/pallas_call | solution.py:105
  186.8 18.7 %shard_map.129 = (f32[2,2048,128]{2,1,0:T(8,128)}, f32[2,2048,256]{2,1,0:T(8,128)}) custom-call(f32[1]{0:T(128)} %dynamic_slice.3.refs_0_, f32[1,128]{1,0:T(1,128)} %bitcast.39, bf16[2048,128]{1,0:T(8,128)(2,1)} %slice.20.refs_2_, bf16[2048,256]{1,0:T(8,128)(2,1)} %collective-permute-done.1.refs_3_, ...), custom_call_target="tpu_custom_call", output_to_operand_aliasing={{0}: (4, {}), {1}: (5, {})} | custom-call | tf_op jit(solution)/shard_map/pallas_call | solution.py:105
  205.6 19.1 %shard_map.130 = bf16[2048,128]{1,0:T(8,128)(2,1)} custom-call(f32[1]{0:T(128)} %dynamic_slice.3.refs_0_, f32[1,128]{1,0:T(1,128)} %bitcast.40, bf16[2048,128]{1,0:T(8,128)(2,1)} %slice.20.refs_2_, bf16[2048,256]{1,0:T(8,128)(2,1)} %collective-permute-done.2.refs_3_, f32[2,2048,128]{2,1,0:T(8,128)} %get-tuple-element.15.refs_4_, ...), custom_call_target="tpu_custom_call" | custom-call | tf_op jit(solution)/shard_map/pallas_call | solution.py:105
  224.7 1.2 copy.32
  225.9 13.6 %all_to_all.11 = bf16[8,256,128]{1,2,0:T(8,128)(2,1)S(1)} all-to-all(bf16[8,256,128]{1,2,0:T(8,128)(2,1)S(1)} %copy.32), channel_id=1, replica_groups={{0,1,2,3,4,5,6,7},{8,9,10,11,12,13,14,15},{16,17,18,19,20,21,22,23},{24..., dimensions={0} | all-to-all | bytes 1048576 | tf_op jit(solution)/shard_map/all_to_all | solution.py:172
  239.5 3.9 %fusion.44 = (f32[256]{0:T(256)S(1)}, f32[256,2048]{1,0:T(8,128)S(1)}) fusion(bf16[256,1024]{0,1:T(8,128)(2,1)S(1)} %bitcast.30, bf16[1024,2048]{1,0:T(8,128)(2,1)} %param.21, bf16[256,2048]{1,0:T(8,128)(2,1)} %param.13), kind=kOutput, calls=%fused_computation.25 | convolution fusion | flops 1075838720 | bytes 7865344 | tf_op jit(solution)/shard_map/dot_general | solution.py:118
  243.8 29.4 %all-gather.2.cloned.1.call-done = bf16[2048,8448]{1,0:T(8,128)(2,1)} async-done(((bf16[64,8448]{1,0:T(8,128)(2,1)}), bf16[2048,8448]{1,0:T(8,128)(2,1)}) %all-gather.2.cloned.1.call-update) | async-done | bytes 34603024 | tf_op jit(solution)/shard_map/all_gather | solution.py:153
  273.2 9.1 %fusion.4 = f32[256,2816]{1,0:T(8,128)} fusion(bf16[2048,8448]{1,0:T(8,128)(2,1)} %all-gather.2.cloned.1.call-done, f32[256,2048]{1,0:T(8,128)S(1)} %get-tuple-element.18, f32[2048]{0:T(1024)S(1)} %copy-done.8, f32[256]{0:T(256)S(1)} %add_rsqrt_fusion, f32[256]{0:T(256)S(1)} %broadcast_multiply_fusion), kind=kOutput, calls=%fused_computation.4 | convolution fusion | flops 2954887168 | bytes 16525312 | tf_op jit(solution)/shard_map/dot_general | solution.py:180
  282.3 13.6 %fusion.37 = bf16[256,2048]{1,0:T(8,128)(2,1)} fusion(bf16[2048,8448]{1,0:T(8,128)(2,1)} %all-gather.2.cloned.1.call-done, f32[256,2816]{1,0:T(8,128)} %fusion.4, f32[2048]{0:T(1024)S(1)} %copy-done.8, f32[256]{0:T(256)S(1)} %add_rsqrt_fusion, f32[256,2048]{1,0:T(8,128)S(1)} %get-tuple-element.18, f32[256]{0:T(256)S(1)} %broadcast_multiply_fusion), kind=kOutput, calls=%fused_computation.16 | convolution fusion | flops 5917769728 | bytes 31215616 | tf_op jit(solution)/shard_map/dot_general | solution.py:183
  (32 shorter events, 1.6 us)
Async XLA Ops:
  6.5 5.7 %copy-start = (bf16[256,1024]{1,0:T(8,128)(2,1)S(1)}, bf16[256,1024]{1,0:T(8,128)(2,1)}, u32[]{:S(2)}) copy-start(bf16[256,1024]{1,0:T(8,128)(2,1)} %param.18) | copy-start | bytes 1572868
  6.5 2.4 copy-start.4
  6.5 266.6 %all-gather.2.cloned.1.call-start = ((), (), s32[]{:S(2)}) async-start(), calls=%async_computation.2 | async-start | bytes 35684352 | tf_op jit(solution)/shard_map/all_gather | solution.py:153
  6.5 2.9 copy-start.5
  9.0 0.9 copy-start.6
  9.0 2.1 copy-start.7
  15.9 133.9 %copy-start.9 = (f32[8]{0:T(128)S(1)}, f32[8]{0:T(128)}, u32[]{:S(2)}) copy-start(f32[8]{0:T(128)} %param.19) | copy-start | bytes 100
  49.7 101.6 %copy-start.2 = (bf16[2048,256]{1,0:T(8,128)(2,1)}, bf16[2048,256]{1,0:T(8,128)(2,1)S(1)}, u32[]{:S(2)}) copy-start(bf16[2048,256]{1,0:T(8,128)(2,1)S(1)} %slice.21.refs_3_) | copy-start | bytes 3145732
  49.7 39.5 %collective-permute-start = (bf16[2048,256]{1,0:T(8,128)(2,1)S(1)}, bf16[2048,256]{1,0:T(8,128)(2,1)S(1)}, u32[]{:S(2)}, u32[]{:S(2)}) collective-permute-start(bf16[2048,256]{1,0:T(8,128)(2,1)S(1)} %slice.21.refs_3_), channel_id=1, source_target_pairs={{0,8},{1,9},{2,10},{3,11},{4,12},{5,13},{6,14},{7,15},{8,16},{9,17... | collective-permute-start | bytes 3145736 | tf_op jit(solution)/shard_map/ppermute | solution.py:169
  89.2 1.0 copy-start.3
  90.1 50.5 %collective-permute-start.1 = (bf16[2048,256]{1,0:T(8,128)(2,1)S(1)}, bf16[2048,256]{1,0:T(8,128)(2,1)}, u32[]{:S(2)}, u32[]{:S(2)}) collective-permute-start(bf16[2048,256]{1,0:T(8,128)(2,1)S(1)} %collective-permute-done.refs_3_), channel_id=1, source_target_pairs={{0,8},{1,9},{2,10},{3,11},{4,12},{5,13},{6,14},{7,15},{8,16},{9,17... | collective-permute-start | bytes 3145736 | tf_op jit(solution)/shard_map/ppermute | solution.py:169
  140.7 64.9 %collective-permute-start.2 = (bf16[2048,256]{1,0:T(8,128)(2,1)}, bf16[2048,256]{1,0:T(8,128)(2,1)}, u32[]{:S(2)}, u32[]{:S(2)}) collective-permute-start(bf16[2048,256]{1,0:T(8,128)(2,1)} %collective-permute-done.1.refs_3_), channel_id=1, source_target_pairs={{0,8},{1,9},{2,10},{3,11},{4,12},{5,13},{6,14},{7,15},{8,16},{9,17... | collective-permute-start | bytes 3145736 | tf_op jit(solution)/shard_map/ppermute | solution.py:169
  243.4 29.8 %copy-start.8 = (f32[2048]{0:T(1024)S(1)}, f32[2048]{0:T(1024)}, u32[]{:S(2)}) copy-start(f32[2048]{0:T(1024)} %param.22) | copy-start | bytes 24580
  282.3 13.6 %copy-start.1 = (bf16[256,1024]{1,0:T(8,128)(2,1)S(1)}, bf16[256,1024]{1,0:T(8,128)(2,1)}, u32[]{:S(2)}) copy-start(bf16[256,1024]{1,0:T(8,128)(2,1)} %param.18) | copy-start | bytes 1572868
Sparse Core Ops, SparseCore 0:
  10.2 262.8 all-gather.1

commit v2 on v1

--- a/solution.py
+++ b/solution.py
@@ -149,8 +149,26 @@
     me = lax.axis_index("sp")
     factor = head_width ** (-0.5)
 
-    packed = jnp.concatenate([gate_weight, up_weight, down_weight.T], axis=1)
-    weights = lax.all_gather(packed, "sp", axis=0, tiled=True)
+    half = hidden_units // 2
+    x_bit, c_bit = lax.rem(me // 2, 2), lax.rem(me, 2)
+    down_rows = down_weight.T
+    halves = [
+        jnp.concatenate([w[:, i * half : (i + 1) * half] for w in (gate_weight, up_weight, down_rows)], axis=1)
+        for i in range(2)
+    ]
+    same, cross = [], []
+    for d in range(group):
+        base, x, c = d - d % 4, d // 2 % 2, d % 2
+        same.append((d, base + 2 * c + x))
+        cross.append((d, base + 2 * (1 - c) + x))
+    got_same = lax.ppermute(jnp.where(c_bit == 0, halves[0], halves[1]), "sp", same)
+    got_cross = lax.ppermute(jnp.where(c_bit == 0, halves[1], halves[0]), "sp", cross)
+    packed = jnp.concatenate(
+        [jnp.where(x_bit == 0, got_same, got_cross), jnp.where(x_bit == 0, got_cross, got_same)], axis=0
+    )
+    alike = [[d for d in range(group) if d // 2 % 2 == x] for x in range(2)]
+    weights = lax.all_gather(packed, "sp", axis=0, axis_index_groups=alike, tiled=True)
+    swap = [(d, d ^ 2) for d in range(group)]
 
     def by_head(a):
         return jnp.transpose(a.reshape(tokens, heads, a.shape[1] // heads), (1, 0, 2))
@@ -164,29 +182,41 @@
     lam = lax.dynamic_slice_in_dim(lambdas, lax.rem(me, heads), 1, 0)
     gain = head_gain.reshape(1, vdim)
     onward = [(d, (d + heads) % group) for d in range(group)]
-    state = None
+    state, other_stream = None, lax.ppermute(stream, "sp", swap)
     for step in range(ring):
         following = lax.ppermute(kv, "sp", onward) if step + 1 < ring else None
         state = attend(lam, gain, q, kv, state, step + 1 == ring, factor)
-        kv = following
+        if following is not None:
+            state, kv, other_stream = lax.optimization_barrier((state, following, other_stream))
     back = lax.all_to_all(
         state.reshape(heads, tokens, vdim), "sp", split_axis=0, concat_axis=0, axis_index_groups=near, tiled=True
     )
     attended = jnp.transpose(back, (1, 0, 2)).reshape(tokens, heads * vdim)
 
-    by_rows = lax.all_to_all(attended, "tp", split_axis=0, concat_axis=1, tiled=True) if tp > 1 else attended
-    own_normed = layer_normed(by_rows, stream, out_weight, norm_gain)
-    normed_all = lax.all_gather(own_normed, "tp", axis=0, tiled=True) if tp > 1 else own_normed
-    gate_out = jnp.dot(normed_all, weights[:, :hidden_units], preferred_element_type=jnp.float32)
-    upward = jnp.dot(normed_all, weights[:, hidden_units : 2 * hidden_units], preferred_element_type=jnp.float32)
-    hidden = (jax.nn.silu(gate_out) * upward).astype(jnp.bfloat16)
-    partial_terms = lax.dot_general(
-        hidden, weights[:, 2 * hidden_units :], (((1,), (1,)), ((), ())), preferred_element_type=jnp.float32
-    ).astype(jnp.bfloat16)
+    other_attended = lax.ppermute(attended, "sp", swap)
+
+    def normed_of(rows, residual):
+        by_rows = lax.all_to_all(rows, "tp", split_axis=0, concat_axis=1, tiled=True) if tp > 1 else rows
+        normed = layer_normed(by_rows, residual, out_weight, norm_gain)
+        return normed, (lax.all_gather(normed, "tp", axis=0, tiled=True) if tp > 1 else normed)
+
+    def mixed(rows):
+        gate_out = jnp.dot(rows, weights[:, :half], preferred_element_type=jnp.float32)
+        upward = jnp.dot(rows, weights[:, half : 2 * half], preferred_element_type=jnp.float32)
+        hidden = (jax.nn.silu(gate_out) * upward).astype(jnp.bfloat16)
+        return lax.dot_general(
+            hidden, weights[:, 2 * half :], (((1,), (1,)), ((), ())), preferred_element_type=jnp.float32
+        )
+
+    own_normed, own_all = normed_of(attended, stream)
+    _, other_all = normed_of(other_attended, other_stream)
+    from_other = lax.ppermute(mixed(other_all).astype(jnp.bfloat16), "sp", swap)
+    partial_terms = lax.optimization_barrier(mixed(own_all)) + from_other.astype(jnp.float32)
     if tp > 1:
-        partial_terms = lax.psum_scatter(partial_terms, "tp", scatter_dimension=0, tiled=True)
-    mixer_out = partial_terms.astype(jnp.float32)
-    return (ALPHA * own_normed.astype(jnp.float32) + 0.5 * mixer_out).astype(jnp.bfloat16)
+        partial_terms = lax.psum_scatter(
+            partial_terms.astype(jnp.bfloat16), "tp", scatter_dimension=0, tiled=True
+        ).astype(jnp.float32)
+    return (ALPHA * own_normed.astype(jnp.float32) + 0.5 * partial_terms).astype(jnp.bfloat16)
 
 
 def solution(mesh):

time: 304 us -> 298 us (0.980)
  blocking collectives: 47.2 us -> 12.4 us
  waiting for transfers between devices: 115 us -> 131 us
  matrix products: 26.6 us -> 35.3 us
  other arithmetic: 2.76 us -> 6.92 us
    all_to_all x1 -> x0, blocking collectives: 33.7 us -> none  [on_device(): lax.all_to_all(own, 'sp', split_axis=0, concat_axis=0, axis_index_groups=...]
    all_gather x1, waiting for transfers between devices: 29.4 us -> 0.01 us  [on_device(): lax.all_gather(packed, 'sp', axis=0, axis_index_groups=alike, tiled=True)]
    ppermute x0 -> x5, waiting for transfers between devices: none -> 28 us  [the longest x1 12 us: on_device(): lax.ppermute(jnp.where(c_bit == 0, halves[1], halves[0]), 'sp', cross)]
    all_to_all x0 -> x1, waiting for transfers between devices: none -> 26.8 us  [on_device(): lax.all_to_all(own, 'sp', split_axis=0, concat_axis=0, axis_index_groups=...]
    ppermute x3, starting transfers between devices: 13.5 us -> 0.01 us  [on_device(): following = lax.ppermute(kv, 'sp', onward) if step + 1 < ring else None]
    ppermute x3, waiting for transfers between devices: 85.7 us -> 76.1 us  [on_device(): following = lax.ppermute(kv, 'sp', onward) if step + 1 < ring else None]
    ppermute x0 -> x5, starting transfers between devices: none -> 8.66 us  [the longest x1 4.21 us: on_device(): lax.ppermute(jnp.where(c_bit == 0, halves[1], halves[0]), 'sp', cross)]
    dot_general x2 -> x4, matrix products: 22.7 us -> 30.2 us  [the longest x2 18.7 us: mixed(): lax.dot_general(hidden, weights[:, 2 * half:], (((1,), (1,)), ((), ())),...]
  transfers between devices with their start and end apart: 4 -> 10, of which waited for: 3 -> 7; matrix products, arithmetic and copies ran while one was open for 5% -> 10% of each run, Pallas kernels for 24% -> 25%
where the time goes in v2:
time: 298 us; the launch traced here: 297 us
  waiting for transfers between devices  131 us (44%)
  Pallas kernels  73.3 us (25%)
  matrix products  35.3 us (12%)
  between operations  13.6 us (5%)
  starting transfers between devices  13.5 us (5%)
  blocking collectives  12.4 us (4%)
  local copies, waits for them, and re-layouts  11.4 us (4%)
  other arithmetic  6.92 us (2%)
    ppermute x3, waiting for transfers between devices, on_device(): following = lax.ppermute(kv, 'sp', onward) if step + 1 < ring else None  76.1 us
    pallas_call x4, Pallas kernels, attend(): pl.pallas_call(functools.partial(attend_kernel, first, last, factor, min(...  73.3 us
    all_to_all x1, waiting for transfers between devices, on_device(): lax.all_to_all(own, 'sp', split_axis=0, concat_axis=0, axis_index_groups=...  26.8 us
    dot_general x2, matrix products, mixed(): lax.dot_general(hidden, weights[:, 2 * half:], (((1,), (1,)), ((), ())),...  18.7 us
    all_to_all x1, blocking collectives, on_device(): lax.all_to_all(state.reshape(heads, tokens, vdim), 'sp', split_axis=0, co...  12.4 us
    ppermute x1, waiting for transfers between devices, on_device(): lax.ppermute(jnp.where(c_bit == 0, halves[1], halves[0]), 'sp', cross)  12 us
    dot_general x2, matrix products, mixed(): jnp.dot(rows, weights[:, :half], preferred_element_type=jnp.float32)  11.5 us
    ppermute x1, waiting for transfers between devices, on_device(): other_attended = lax.ppermute(attended, 'sp', swap)  8.46 us
  transfers between devices with their start and end apart: 10, of which 7 were waited for; matrix products, arithmetic and copies ran while one was open for 10% of the time, Pallas kernels for 25%

profile of v2, /device:TPU:0, one launch (start us, length us, event | category | flops | bytes accessed | tf_op | source)
XLA Modules:
  0.0 297.3 jit_solution(13182319293642971671)
XLA Ops:
  9.8 4.2 %collective-permute-start.5 = (bf16[64,4224]{1,0:T(8,128)(2,1)S(1)}, bf16[64,4224]{1,0:T(8,128)(2,1)S(1)}, u32[]{:S(2)}, u32[]{:S(2)}) collective-permute-start(bf16[64,4224]{1,0:T(8,128)(2,1)S(1)} %get-tuple-element.44), channel_id=1, source_target_pairs={{0,2},{1,0},{2,3},{3,1},{4,6},{5,4},{6,7},{7,5},{8,10},{9,8},{10,1... | collective-permute-start | bytes 1622024 | tf_op jit(solution)/shard_map/ppermute | solution.py:165
  14.0 12.0 %collective-permute-done.5 = bf16[64,4224]{1,0:T(8,128)(2,1)S(1)} collective-permute-done((bf16[64,4224]{1,0:T(8,128)(2,1)S(1)}, bf16[64,4224]{1,0:T(8,128)(2,1)S(1)}, u32[]{:S(2)}, u32[]{:S(2)}) %collective-permute-start.5) | collective-permute-done | bytes 540704 | tf_op jit(solution)/shard_map/ppermute | solution.py:165
  29.2 2.3 concatenate.12
  31.5 4.8 %all-to-all-start = ((bf16[8,256,384]{2,1,0:T(8,128)(2,1)}), bf16[8,256,384]{2,1,0:T(8,128)(2,1)S(1)}, u32[]{:S(2)}, u32[]{:S(2)}) async-start(bf16[8,256,384]{2,1,0:T(8,128)(2,1)} %concatenate.12), calls=%async_computation | async-start | bytes 3145728 | tf_op jit(solution)/shard_map/all_to_all | solution.py:178
  36.3 2.0 collective-permute-start.1
  38.3 26.8 %all-to-all-done = bf16[8,256,384]{2,1,0:T(8,128)(2,1)S(1)} async-done(((bf16[8,256,384]{2,1,0:T(8,128)(2,1)}), bf16[8,256,384]{2,1,0:T(8,128)(2,1)S(1)}, u32[]{:S(2)}, u32[]{:S(2)}) %all-to-all-start) | async-done | bytes 1572896 | tf_op jit(solution)/shard_map/all_to_all | solution.py:178
  67.6 16.8 %shard_map.127 = (f32[2,2048,128]{2,1,0:T(8,128)}, f32[2,2048,256]{2,1,0:T(8,128)}) custom-call(f32[1]{0:T(128)} %dynamic_slice.3.refs_0_, f32[1,128]{1,0:T(1,128)} %bitcast.44, bf16[2048,128]{1,0:T(8,128)(2,1)} %slice.47.refs_2_, bf16[2048,256]{1,0:T(8,128)(2,1)} %slice.48.refs_3_), custom_call_target="tpu_custom_call" | custom-call | tf_op jit(solution)/shard_map/pallas_call | solution.py:105
  84.4 31.6 %collective-permute-done.refs_3_ = bf16[2048,256]{1,0:T(8,128)(2,1)} collective-permute-done((bf16[2048,256]{1,0:T(8,128)(2,1)}, bf16[2048,256]{1,0:T(8,128)(2,1)}, u32[]{:S(2)}, u32[]{:S(2)}) %collective-permute-start) | collective-permute-done | bytes 1048608 | tf_op jit(solution)/shard_map/ppermute | solution.py:187
  115.9 18.8 %shard_map.128 = (f32[2,2048,128]{2,1,0:T(8,128)}, f32[2,2048,256]{2,1,0:T(8,128)}) custom-call(f32[1]{0:T(128)} %dynamic_slice.3.refs_0_, f32[1,128]{1,0:T(1,128)} %bitcast.45, bf16[2048,128]{1,0:T(8,128)(2,1)} %slice.47.refs_2_, bf16[2048,256]{1,0:T(8,128)(2,1)} %collective-permute-done.refs_3_, ...), custom_call_target="tpu_custom_call", output_to_operand_aliasing={{0}: (4, {}), {1}: (5, {})} | custom-call | tf_op jit(solution)/shard_map/pallas_call | solution.py:105
  134.8 30.7 %collective-permute-done.2.refs_3_ = bf16[2048,256]{1,0:T(8,128)(2,1)S(1)} collective-permute-done((bf16[2048,256]{1,0:T(8,128)(2,1)}, bf16[2048,256]{1,0:T(8,128)(2,1)S(1)}, u32[]{:S(2)}, u32[]{:S(2)}) %collective-permute-start.2) | collective-permute-done | bytes 1048608 | tf_op jit(solution)/shard_map/ppermute | solution.py:187
  166.5 18.7 %shard_map.129 = (f32[2,2048,128]{2,1,0:T(8,128)}, f32[2,2048,256]{2,1,0:T(8,128)}) custom-call(f32[1]{0:T(128)} %dynamic_slice.3.refs_0_, f32[1,128]{1,0:T(1,128)} %bitcast.46, bf16[2048,128]{1,0:T(8,128)(2,1)} %slice.47.refs_2_, bf16[2048,256]{1,0:T(8,128)(2,1)} %copy-done.3, ...), custom_call_target="tpu_custom_call", output_to_operand_aliasing={{0}: (4, {}), {1}: (5, {})} | custom-call | tf_op jit(solution)/shard_map/pallas_call | solution.py:105
  185.1 13.8 %collective-permute-done.3.refs_3_ = bf16[2048,256]{1,0:T(8,128)(2,1)} collective-permute-done((bf16[2048,256]{1,0:T(8,128)(2,1)S(1)}, bf16[2048,256]{1,0:T(8,128)(2,1)}, u32[]{:S(2)}, u32[]{:S(2)}) %collective-permute-start.3) | collective-permute-done | bytes 1048608 | tf_op jit(solution)/shard_map/ppermute | solution.py:187
  198.9 19.0 %shard_map.130 = bf16[2048,128]{1,0:T(8,128)(2,1)} custom-call(f32[1]{0:T(128)} %dynamic_slice.3.refs_0_, f32[1,128]{1,0:T(1,128)} %bitcast.47, bf16[2048,128]{1,0:T(8,128)(2,1)} %slice.47.refs_2_, bf16[2048,256]{1,0:T(8,128)(2,1)} %collective-permute-done.3.refs_3_, f32[2,2048,128]{2,1,0:T(8,128)} %get-tuple-element.38.refs_4_, ...), custom_call_target="tpu_custom_call" | custom-call | tf_op jit(solution)/shard_map/pallas_call | solution.py:105
  219.2 12.4 %all_to_all.10 = bf16[8,256,128]{1,2,0:T(8,128)(2,1)S(1)} all-to-all(bf16[8,256,128]{1,2,0:T(8,128)(2,1)S(1)} %copy.32), channel_id=1, replica_groups={{0,1,2,3,4,5,6,7},{8,9,10,11,12,13,14,15},{16,17,18,19,20,21,22,23},{24..., dimensions={0} | all-to-all | bytes 1048576 | tf_op jit(solution)/shard_map/all_to_all | solution.py:191
  232.2 3.7 %fusion.49 = (f32[256]{0:T(256)S(1)}, f32[256,2048]{1,0:T(8,128)S(1)}) fusion(bf16[256,1024]{0,1:T(8,128)(2,1)S(1)} %bitcast.37, bf16[1024,2048]{1,0:T(8,128)(2,1)} %param.21, bf16[256,2048]{1,0:T(8,128)(2,1)S(1)} %copy-done.2), kind=kOutput, calls=%fused_computation.54 | convolution fusion | flops 1075838720 | bytes 7865344 | tf_op jit(solution)/shard_map/dot_general | solution.py:118
  236.3 8.5 %collective-permute-done.6 = bf16[256,1024]{0,1:T(8,128)(2,1)S(1)} collective-permute-done((bf16[256,1024]{0,1:T(8,128)(2,1)S(1)}, bf16[256,1024]{0,1:T(8,128)(2,1)S(1)}, u32[]{:S(2)}, u32[]{:S(2)}) %collective-permute-start.6) | collective-permute-done | bytes 524320 | tf_op jit(solution)/shard_map/ppermute | solution.py:196
  244.8 1.4 fusion.43
  246.8 1.7 multiply_convert_fusion
  248.5 6.0 %fusion.8 = f32[256,1408]{1,0:T(8,128)} fusion(bf16[256,2048]{1,0:T(8,128)(2,1)} %get-tuple-element.51, bf16[2048,4224]{1,0:T(8,128)(2,1)} %all-gather.2.cloned.1.call-done), kind=kOutput, calls=%fused_computation.8 | convolution fusion | flops 1476395008 | bytes 8257536 | tf_op jit(solution)/shard_map/dot_general | solution.py:204
  254.5 9.2 %fusion.24 = bf16[256,2048]{1,0:T(8,128)(2,1)} fusion(bf16[2048,4224]{1,0:T(8,128)(2,1)} %all-gather.2.cloned.1.call-done, bf16[256,2048]{1,0:T(8,128)(2,1)S(1)} %copy-done.4, f32[256,1408]{1,0:T(8,128)} %fusion.8), kind=kOutput, calls=%fused_computation.17 | convolution fusion | flops 2955476992 | bytes 15073280 | tf_op jit(solution)/shard_map/dot_general | solution.py:207
  264.8 5.6 %fusion.10 = f32[256,1408]{1,0:T(8,128)} fusion(bf16[256,2048]{1,0:T(8,128)(2,1)S(1)} %get-tuple-element.52, bf16[2048,4224]{1,0:T(8,128)(2,1)} %all-gather.2.cloned.1.call-done), kind=kOutput, calls=%fused_computation.10 | convolution fusion | flops 1476395008 | bytes 8257536 | tf_op jit(solution)/shard_map/dot_general | solution.py:204
  270.4 9.5 %fusion.2 = f32[256,2048]{1,0:T(8,128)} fusion(bf16[2048,4224]{1,0:T(8,128)(2,1)} %all-gather.2.cloned.1.call-done, bf16[256,2048]{1,0:T(8,128)(2,1)S(1)} %get-tuple-element.52, f32[256,1408]{1,0:T(8,128)} %fusion.10), kind=kOutput, calls=%fused_computation.2 | convolution fusion | flops 2954952704 | bytes 16121856 | tf_op jit(solution)/shard_map/dot_general | solution.py:207
  279.9 7.5 %collective-permute-done.7 = bf16[256,2048]{1,0:T(8,128)(2,1)S(1)} collective-permute-done((bf16[256,2048]{1,0:T(8,128)(2,1)}, bf16[256,2048]{1,0:T(8,128)(2,1)S(1)}, u32[]{:S(2)}, u32[]{:S(2)}) %collective-permute-start.7) | collective-permute-done | bytes 1048608 | tf_op jit(solution)/shard_map/ppermute | solution.py:213
  287.4 3.0 %add_convert_fusion = bf16[256,2048]{1,0:T(8,128)(2,1)} fusion(f32[256,2048]{1,0:T(8,128)} %fusion.2, bf16[256,2048]{1,0:T(8,128)(2,1)S(1)} %collective-permute-done.7, bf16[256,2048]{1,0:T(8,128)(2,1)S(1)} %get-tuple-element.52), kind=kLoop, calls=%fused_computation.18 | loop fusion | flops 3670016 | bytes 5242880 | tf_op jit(solution)/shard_map/convert_element_type | solution.py:219
  (57 shorter events, 13.8 us)
Async XLA Ops:
  6.5 22.5 %copy-start = (bf16[256,1024]{1,0:T(8,128)(2,1)S(1)}, bf16[256,1024]{1,0:T(8,128)(2,1)}, u32[]{:S(2)}) copy-start(bf16[256,1024]{1,0:T(8,128)(2,1)} %param.18) | copy-start | bytes 1572868
  6.5 242.0 %all-gather.2.cloned.1.call-start = ((), (), s32[]{:S(2)}) async-start(), calls=%async_computation.2 | async-start | bytes 18382848 | tf_op jit(solution)/shard_map/all_gather | solution.py:170
  9.1 4.9 %collective-permute-start.4 = (bf16[64,4224]{1,0:T(8,128)(2,1)S(1)}, bf16[64,4224]{1,0:T(8,128)(2,1)S(1)}, u32[]{:S(2)}, u32[]{:S(2)}) collective-permute-start(bf16[64,4224]{1,0:T(8,128)(2,1)S(1)} %get-tuple-element.43), channel_id=1, source_target_pairs={{0,0},{1,2},{2,1},{3,3},{4,4},{5,6},{6,5},{7,7},{8,8},{9,10},{10,9... | collective-permute-start | bytes 1622024 | tf_op jit(solution)/shard_map/ppermute | solution.py:164
  9.8 16.3 %collective-permute-start.5 = (bf16[64,4224]{1,0:T(8,128)(2,1)S(1)}, bf16[64,4224]{1,0:T(8,128)(2,1)S(1)}, u32[]{:S(2)}, u32[]{:S(2)}) collective-permute-start(bf16[64,4224]{1,0:T(8,128)(2,1)S(1)} %get-tuple-element.44), channel_id=1, source_target_pairs={{0,2},{1,0},{2,3},{3,1},{4,6},{5,4},{6,7},{7,5},{8,10},{9,8},{10,1... | collective-permute-start | bytes 1622024 | tf_op jit(solution)/shard_map/ppermute | solution.py:165
  26.1 1.1 copy-start.5
  26.2 1.5 copy-start.6
  27.2 1.0 copy-start.7
  27.3 1.4 copy-start.8
  31.5 34.7 %copy-start.10 = (f32[8]{0:T(128)S(1)}, f32[8]{0:T(128)}, u32[]{:S(2)}) copy-start(f32[8]{0:T(128)} %param.19) | copy-start | bytes 100
  31.5 33.7 %all-to-all-start = ((bf16[8,256,384]{2,1,0:T(8,128)(2,1)}), bf16[8,256,384]{2,1,0:T(8,128)(2,1)S(1)}, u32[]{:S(2)}, u32[]{:S(2)}) async-start(bf16[8,256,384]{2,1,0:T(8,128)(2,1)} %concatenate.12), calls=%async_computation | async-start | bytes 3145728 | tf_op jit(solution)/shard_map/all_to_all | solution.py:178
  36.3 48.1 %collective-permute-start.1 = (bf16[256,2048]{1,0:T(8,128)(2,1)}, bf16[256,2048]{1,0:T(8,128)(2,1)S(1)}, u32[]{:S(2)}, u32[]{:S(2)}) collective-permute-start(bf16[256,2048]{1,0:T(8,128)(2,1)} %param.13), channel_id=1, source_target_pairs={{0,2},{1,3},{2,0},{3,1},{4,6},{5,7},{6,4},{7,5},{8,10},{9,11},{10,... | collective-permute-start | bytes 3145736 | tf_op jit(solution)/shard_map/ppermute | solution.py:185
  66.2 49.7 %collective-permute-start = (bf16[2048,256]{1,0:T(8,128)(2,1)}, bf16[2048,256]{1,0:T(8,128)(2,1)}, u32[]{:S(2)}, u32[]{:S(2)}) collective-permute-start(bf16[2048,256]{1,0:T(8,128)(2,1)} %slice.48.refs_3_), channel_id=1, source_target_pairs={{0,8},{1,9},{2,10},{3,11},{4,12},{5,13},{6,14},{7,15},{8,16},{9,17... | collective-permute-start | bytes 3145736 | tf_op jit(solution)/shard_map/ppermute | solution.py:187
  115.9 49.6 %collective-permute-start.2 = (bf16[2048,256]{1,0:T(8,128)(2,1)}, bf16[2048,256]{1,0:T(8,128)(2,1)S(1)}, u32[]{:S(2)}, u32[]{:S(2)}) collective-permute-start(bf16[2048,256]{1,0:T(8,128)(2,1)} %collective-permute-done.refs_3_), channel_id=1, source_target_pairs={{0,8},{1,9},{2,10},{3,11},{4,12},{5,13},{6,14},{7,15},{8,16},{9,17... | collective-permute-start | bytes 3145736 | tf_op jit(solution)/shard_map/ppermute | solution.py:187
  165.5 1.0 copy-start.3
  165.5 33.4 %collective-permute-start.3 = (bf16[2048,256]{1,0:T(8,128)(2,1)S(1)}, bf16[2048,256]{1,0:T(8,128)(2,1)}, u32[]{:S(2)}, u32[]{:S(2)}) collective-permute-start(bf16[2048,256]{1,0:T(8,128)(2,1)S(1)} %collective-permute-done.2.refs_3_), channel_id=1, source_target_pairs={{0,8},{1,9},{2,10},{3,11},{4,12},{5,13},{6,14},{7,15},{8,16},{9,17... | collective-permute-start | bytes 3145736 | tf_op jit(solution)/shard_map/ppermute | solution.py:187
  217.9 14.3 %copy-start.2 = (bf16[256,2048]{1,0:T(8,128)(2,1)S(1)}, bf16[256,2048]{1,0:T(8,128)(2,1)}, u32[]{:S(2)}) copy-start(bf16[256,2048]{1,0:T(8,128)(2,1)} %param.13) | copy-start | bytes 3145732
  231.7 13.1 %collective-permute-start.6 = (bf16[256,1024]{0,1:T(8,128)(2,1)S(1)}, bf16[256,1024]{0,1:T(8,128)(2,1)S(1)}, u32[]{:S(2)}, u32[]{:S(2)}) collective-permute-start(bf16[256,1024]{0,1:T(8,128)(2,1)S(1)} %bitcast.36), channel_id=1, source_target_pairs={{0,2},{1,3},{2,0},{3,1},{4,6},{5,7},{6,4},{7,5},{8,10},{9,11},{10,... | collective-permute-start | bytes 1572872 | tf_op jit(solution)/shard_map/ppermute | solution.py:196
  232.2 12.5 %copy-start.1 = (bf16[1024,2048]{1,0:T(8,128)(2,1)S(1)}, bf16[1024,2048]{1,0:T(8,128)(2,1)}, u32[]{:S(2)}) copy-start(bf16[1024,2048]{1,0:T(8,128)(2,1)} %param.21) | copy-start | bytes 12582916
  246.1 0.7 copy-start.9
  248.5 6.0 %copy-start.4 = (bf16[256,2048]{1,0:T(8,128)(2,1)S(1)}, bf16[256,2048]{1,0:T(8,128)(2,1)}, u32[]{:S(2)}) copy-start(bf16[256,2048]{1,0:T(8,128)(2,1)} %get-tuple-element.51) | copy-start | bytes 3145732
  263.7 23.7 %collective-permute-start.7 = (bf16[256,2048]{1,0:T(8,128)(2,1)}, bf16[256,2048]{1,0:T(8,128)(2,1)S(1)}, u32[]{:S(2)}, u32[]{:S(2)}) collective-permute-start(bf16[256,2048]{1,0:T(8,128)(2,1)} %fusion.24), channel_id=1, source_target_pairs={{0,2},{1,3},{2,0},{3,1},{4,6},{5,7},{6,4},{7,5},{8,10},{9,11},{10,... | collective-permute-start | bytes 3145736 | tf_op jit(solution)/shard_map/ppermute | solution.py:213
Sparse Core Ops, SparseCore 0:
  27.4 153.1 all-gather.1
